TPU v7x, 32 devices: a whole 2x2x4 slice. The times are simulated.
32 devices in a mesh: kv: 4 (over y, x), tp: 8 (over z, core).
Axes of the slice: x: 2, y: 2, z: 4, core: 2. Of those that a mesh axis runs over, the one named last changes fastest.
Arguments:
- tokens: bfloat16 [128, 4096], P(None, 'tp'), may hold values from -6 to 6
- norm_gain: float32 [4096], P('tp'), may hold values from 0.1 to 1.9
- query_weight: bfloat16 [4096, 2048], P('tp', 'kv'), may hold values from -0.09375 to 0.09375
- key_weight: bfloat16 [4096, 2048], P('tp', 'kv'), may hold values from -0.09375 to 0.09375
- value_weight: bfloat16 [4096, 2048], P('tp', 'kv'), may hold values from -0.09375 to 0.09375
- input_gate_weight: bfloat16 [4096, 16], P('tp'), may hold values from -0.09375 to 0.09375
- forget_gate_weight: bfloat16 [4096, 16], P('tp'), may hold values from -0.09375 to 0.09375
- input_gate_bias: float32 [16], P('kv'), may hold values from -2 to 2
- forget_gate_bias: float32 [16], P('kv'), may hold values from 1 to 6
- memory_state: float32 [128, 16, 128, 128], P('tp', 'kv'), may hold values from -12 to 12
- normalizer_state: float32 [128, 16, 128], P('tp', 'kv'), may hold values from -24 to 24
- stabilizer_state: float32 [128, 16], P('tp', 'kv'), may hold values from -1 to 3
- block_keys: bfloat16 [128, 16, 128, 128], P('tp', 'kv'), may hold values from -6 to 6
- block_values: bfloat16 [128, 16, 128, 128], P('tp', 'kv'), may hold values from -6 to 6
- block_input_pre: float32 [128, 16, 128], P('tp', 'kv'), may hold values from -6 to 6
- block_forget_pre: float32 [128, 16, 128], P('tp', 'kv'), may hold values from -6 to 6
- block_lengths: int32 [128], P('tp'), may hold values from 1 to 128, 6553 in all
- head_norm_gain: float32 [2048], P('kv'), may hold values from 0.1 to 1.9
- output_weight: bfloat16 [2048, 4096], P('kv', 'tp'), may hold values from -0.125 to 0.125
- mixer_norm_gain: float32 [4096], P('tp'), may hold values from 0.1 to 1.9
- gate_weight: bfloat16 [4096, 11264], P('tp', 'kv'), may hold values from -0.09375 to 0.09375
- up_weight: bfloat16 [4096, 11264], P('tp', 'kv'), may hold values from -0.09375 to 0.09375
- down_weight: bfloat16 [11264, 4096], P('kv', 'tp'), may hold values from -0.0546875 to 0.0546875
Outputs:
- layer_output: float32 [128, 4096], P(None, 'tp')
Inputs may be any that keep to these rules, and one draw needn't show every extreme that they name: `block_lengths`: some sequence has exactly 128 live positions.
All inputs are finite; a program needn't handle non-finite values. No bound on the sum of `block_lengths` on one device may be relied on, other than what follows from the above.
Results may differ from a plain program's by a relative error of at most 0.0078.
Values may be sent and summed in bfloat16 or wider, within the bound.
No kernel may reach another device: no remote copies, remote signals or barrier semaphores. Data moves between devices by JAX's collectives and lax.ppermute only.
A program may use at most 64 MiB of HBM per device.

v0:
```python
import jax
import jax.numpy as jnp
from jax import lax
from jax.sharding import PartitionSpec as P

D = 4096
epsilon = 1e-06


def memory_cell(
    queries,
    new_keys,
    new_values,
    log_input,
    log_forget,
    memory,
    normalizer,
    stabilizer,
    cached_keys,
    cached_values,
    input_pre,
    forget_pre,
    lengths,
    input_bias,
    forget_bias,
):
    positions = jnp.arange(cached_keys.shape[2])
    is_live = (positions[None, :] < lengths[:, None])[:, None, :]
    cached_input = input_pre + input_bias[None, :, None]
    cached_forget = jnp.where(
        is_live, jax.nn.log_sigmoid(forget_pre + forget_bias[None, :, None]), 0.0
    )
    after_mask = (positions[:, None] > positions[None, :]).astype(jnp.float32)
    later_forget = (
        jnp.einsum("bhu,us->bhs", cached_forget, after_mask, precision=lax.Precision.HIGHEST)
        + log_forget[..., None]
    )
    total_forget = jnp.sum(cached_forget, axis=-1) + log_forget
    exponent = jnp.where(is_live, later_forget + cached_input, -jnp.inf)
    carried = total_forget + stabilizer
    stab_max = jnp.maximum(jnp.maximum(jnp.max(exponent, axis=-1), carried), log_input)
    scores = jnp.einsum("bhd,bhsd->bhs", queries, cached_keys, preferred_element_type=jnp.float32)
    block_weight = jnp.exp(exponent - stab_max[..., None]) * scores
    block_probs = block_weight.astype(jnp.bfloat16)
    block_sum = jnp.einsum(
        "bhs,bhsd->bhd", block_probs, cached_values, preferred_element_type=jnp.float32
    )
    query_wide = queries.astype(jnp.float32)
    new_weight = jnp.exp(log_input - stab_max) * jnp.sum(
        query_wide * new_keys.astype(jnp.float32), axis=-1
    )
    state_weight = jnp.exp(carried - stab_max)
    state_sum = jnp.einsum("bhkv,bhk->bhv", memory, query_wide, precision=lax.Precision.HIGHEST)
    state_norm = jnp.sum(normalizer * query_wide, axis=-1)
    numerator = (
        block_sum
        + new_weight[..., None] * new_values.astype(jnp.float32)
        + state_weight[..., None] * state_sum
    )
    denominator = jnp.sum(block_weight, axis=-1) + new_weight + state_weight * state_norm
    return numerator / jnp.maximum(jnp.abs(denominator), 1.0)[..., None]


def head_scale(cell_out, gain):
    return (cell_out * gain.reshape(cell_out.shape[1], cell_out.shape[2])).astype(jnp.bfloat16)


def activate(gate_sum, up_sum, square_sum):
    row_scale = lax.rsqrt(square_sum / D + epsilon)[:, None]
    return (jax.nn.silu(gate_sum * row_scale) * (up_sum * row_scale)).astype(jnp.bfloat16)


def body(
    tokens,
    norm_gain,
    query_weight,
    key_weight,
    value_weight,
    input_gate_weight,
    forget_gate_weight,
    input_gate_bias,
    forget_gate_bias,
    memory_state,
    normalizer_state,
    stabilizer_state,
    block_keys,
    block_values,
    block_input_pre,
    block_forget_pre,
    block_lengths,
    head_norm_gain,
    output_weight,
    mixer_norm_gain,
    gate_weight,
    up_weight,
    down_weight,
):
    seq_rows = block_keys.shape[0]
    heads_dev = block_keys.shape[1]
    head_size = block_keys.shape[3]
    tok_wide = tokens.astype(jnp.float32)
    scaled_in = (tok_wide * norm_gain).astype(jnp.bfloat16)
    square_part = jnp.sum(tok_wide * tok_wide, axis=1)

    def partial_of(weight):
        return jnp.dot(scaled_in, weight, preferred_element_type=jnp.float32)

    query_sum, key_sum, value_sum, input_sum, forget_sum, square_sum = (
        lax.psum_scatter(partial_of(query_weight), "tp", scatter_dimension=0, tiled=True),
        lax.psum_scatter(partial_of(key_weight), "tp", scatter_dimension=0, tiled=True),
        lax.psum_scatter(partial_of(value_weight), "tp", scatter_dimension=0, tiled=True),
        lax.psum_scatter(partial_of(input_gate_weight), "tp", scatter_dimension=0, tiled=True),
        lax.psum_scatter(partial_of(forget_gate_weight), "tp", scatter_dimension=0, tiled=True),
        lax.psum_scatter(square_part, "tp", scatter_dimension=0, tiled=True),
    )
    first_scale = lax.rsqrt(square_sum / D + epsilon)[:, None]
    queries = (
        (query_sum * first_scale * head_size ** (-0.5))
        .astype(jnp.bfloat16)
        .reshape(seq_rows, heads_dev, head_size)
    )
    new_keys = (key_sum * first_scale).astype(jnp.bfloat16).reshape(seq_rows, heads_dev, head_size)
    new_values = (
        (value_sum * first_scale).astype(jnp.bfloat16).reshape(seq_rows, heads_dev, head_size)
    )
    head_start = lax.axis_index("kv") * heads_dev
    log_input = (
        lax.dynamic_slice_in_dim(input_sum * first_scale, head_start, heads_dev, 1)
        + input_gate_bias
    )
    log_forget = jax.nn.log_sigmoid(
        lax.dynamic_slice_in_dim(forget_sum * first_scale, head_start, heads_dev, 1)
        + forget_gate_bias
    )
    cell_out = memory_cell(
        queries,
        new_keys,
        new_values,
        log_input,
        log_forget,
        memory_state,
        normalizer_state,
        stabilizer_state,
        block_keys,
        block_values,
        block_input_pre,
        block_forget_pre,
        block_lengths,
        input_gate_bias,
        forget_gate_bias,
    )
    head_out = head_scale(cell_out, head_norm_gain).reshape(seq_rows, heads_dev * head_size)
    attended_part = jnp.dot(
        lax.all_gather(head_out, "tp", axis=0, tiled=True),
        output_weight,
        preferred_element_type=jnp.float32,
    )
    attended = lax.psum(attended_part, "kv")
    res_wide = tok_wide + attended
    mid_square = jnp.sum(res_wide * res_wide, axis=1)
    mid_scaled = (res_wide * mixer_norm_gain).astype(jnp.bfloat16)
    gate_part = jnp.dot(mid_scaled, gate_weight, preferred_element_type=jnp.float32)
    up_part = jnp.dot(mid_scaled, up_weight, preferred_element_type=jnp.float32)
    gate_sum, up_sum, mid_sum = lax.psum((gate_part, up_part, mid_square), "tp")
    hidden = activate(gate_sum, up_sum, mid_sum)
    down_part = jnp.dot(hidden, down_weight, preferred_element_type=jnp.float32)
    mixed = lax.psum(down_part, "kv")
    return res_wide + mixed


def solution(mesh):
    placed = (
        P(None, "tp"),
        P("tp"),
        P("tp", "kv"),
        P("tp", "kv"),
        P("tp", "kv"),
        P("tp", None),
        P("tp", None),
        P("kv"),
        P("kv"),
        P("tp", "kv", None, None),
        P("tp", "kv", None),
        P("tp", "kv"),
        P("tp", "kv", None, None),
        P("tp", "kv", None, None),
        P("tp", "kv", None),
        P("tp", "kv", None),
        P("tp"),
        P("kv"),
        P("kv", "tp"),
        P("tp"),
        P("tp", "kv"),
        P("tp", "kv"),
        P("kv", "tp"),
    )
    return jax.shard_map(body, mesh=mesh, in_specs=placed, out_specs=P(None, "tp"), check_vma=False)
```

profile of v0, /device:TPU:0, one launch (start us, length us, event | category | flops | bytes accessed | tf_op | source)
XLA Modules:
  0.0 376.3 jit_solution(17206025061885807073)
XLA Ops:
  6.6 1.9 fusion.16
  8.5 1.7 fusion.14
  10.3 2.1 fusion.12
  12.5 2.1 fusion.10
  15.8 18.1 %all-reduce = f32[128]{0:T(128)S(1)} all-reduce(f32[128]{0:T(128)S(1)} %fusion.4), channel_id=3, replica_groups=mesh['kv'=4,'tp'=8] {'tp'}, use_global_device_ids=true, to_apply=%region_2.0.clone | all-reduce | flops 128 | bytes 1024
  37.7 5.3 %reduce-scatter.16.cloned.1.call-done = f32[16,16]{1,0:T(8,128)} async-done(((f32[128,16]{1,0:T(8,128)}), f32[16,16]{1,0:T(8,128)}) %reduce-scatter.16.cloned.1.call-update) | async-done | bytes 1040
  43.9 29.9 %reduce-scatter.18.cloned.1.call-done = f32[16,16]{1,0:T(8,128)} async-done(((f32[128,16]{1,0:T(8,128)}), f32[16,16]{1,0:T(8,128)}) %reduce-scatter.18.cloned.1.call-update) | async-done | bytes 1040
  74.6 1.6 fusion.34
  76.9 27.9 %reduce-scatter.10.cloned.1.call-done = f32[16,512]{1,0:T(8,128)} async-done(((f32[128,512]{1,0:T(8,128)}), f32[16,512]{1,0:T(8,128)}) %reduce-scatter.10.cloned.1.call-update) | async-done | bytes 32784 | tf_op jit(solution)/shard_map/reduce_scatter | solution.py:109
  104.9 31.1 %reduce-scatter.12.cloned.1.call-done = f32[16,512]{1,0:T(8,128)} async-done(((f32[128,512]{1,0:T(8,128)}), f32[16,512]{1,0:T(8,128)}) %reduce-scatter.12.cloned.1.call-update) | async-done | bytes 32784 | tf_op jit(solution)/shard_map/reduce_scatter | solution.py:110
  136.0 31.1 %reduce-scatter.14.cloned.1.call-done = f32[16,512]{1,0:T(8,128)} async-done(((f32[128,512]{1,0:T(8,128)}), f32[16,512]{1,0:T(8,128)}) %reduce-scatter.14.cloned.1.call-update) | async-done | bytes 32784 | tf_op jit(solution)/shard_map/reduce_scatter | solution.py:111
  167.0 1.5 fusion.25
  170.8 4.9 %fusion.36 = f32[16,4,1,128]{3,2,1,0:T(1,128)} fusion(bf16[16,4,128,1]{2,3,1,0:T(2,128)(2,1)S(1)} %reshape.54, f32[16,4,128,128]{3,2,1,0:T(8,128)} %param.32), kind=kOutput, calls=%fused_computation.61 | convolution fusion | flops 12582912 | bytes 4243456 | tf_op jit(solution)/shard_map/bhkv,bhk->bhv/dot_general | solution.py:53
  175.8 2.0 fusion.35
  184.2 2.3 fusion.22
  186.7 14.0 %all_gather.3 = bf16[128,512]{1,0:T(8,128)(2,1)S(1)} all-gather(bf16[16,512]{1,0:T(8,128)(2,1)S(1)} %bitcast.45), channel_id=1, replica_groups=mesh['kv'=4,'tp'=8] {'tp'}, dimensions={0}, use_global_device_ids=true | all-gather | bytes 147456 | tf_op jit(solution)/shard_map/all_gather | solution.py:154
  201.7 41.3 %all-reduce.6.cloned.1.call-done = f32[128,512]{1,0:T(8,128)} async-done(((f32[128,512]{1,0:T(8,128)}), f32[128,512]{1,0:T(8,128)}) %all-reduce.6.cloned.1.call-update) | async-done | bytes 262160 | tf_op jit(solution)/shard_map/psum | solution.py:158
  244.1 1.7 fusion.39
  246.4 1.7 fusion.38
  248.2 16.2 %psum.37 = f32[128]{0:T(128)S(1)} all-reduce(f32[128]{0:T(128)S(1)} %get-tuple-element.12), channel_id=1, replica_groups=mesh['kv'=4,'tp'=8] {'tp'}, use_global_device_ids=true, to_apply=%region_15.16 | all-reduce | flops 128 | bytes 1024 | tf_op jit(solution)/shard_map/psum | solution.py:164
  264.4 56.5 %all-reduce.10.cloned.1.call-done = (f32[128,2816]{1,0:T(8,128)}, f32[128,2816]{1,0:T(8,128)}) async-done(((f32[128,2816]{1,0:T(8,128)}, f32[128,2816]{1,0:T(8,128)}), (f32[128,2816]{1,0:T(8,128)}, f32[128,2816]{1,0:T(8,128)})) %all-reduce.10.cloned.1.call-update) | async-done | bytes 2883600 | tf_op jit(solution)/shard_map/psum | solution.py:164
  320.9 4.2 %fusion.2 = f32[128,512]{1,0:T(8,128)} fusion(bf16[2816,512]{1,0:T(8,128)(2,1)} %param.45, f32[128,2816]{1,0:T(8,128)} %get-tuple-element.7, f32[128,2816]{1,0:T(8,128)} %get-tuple-element.8, f32[128]{0:T(128)S(1)} %add_rsqrt_fusion), kind=kOutput, calls=%fused_computation.4 | convolution fusion | flops 371982336 | bytes 6029824 | tf_op jit(solution)/shard_map/dot_general | solution.py:166
  325.1 42.7 %all-reduce.8.cloned.1.call-done = f32[128,512]{1,0:T(8,128)} async-done(((f32[128,512]{1,0:T(8,128)}), f32[128,512]{1,0:T(8,128)}) %all-reduce.8.cloned.1.call-update) | async-done | bytes 262160 | tf_op jit(solution)/shard_map/psum | solution.py:167
  367.8 1.7 fusion.5
  (111 shorter events, 18.5 us)
Async XLA Ops:
  6.5 237.5 %copy-start = (bf16[512,2816]{1,0:T(8,128)(2,1)S(1)}, bf16[512,2816]{1,0:T(8,128)(2,1)}, u32[]{:S(2)}) copy-start(bf16[512,2816]{1,0:T(8,128)(2,1)} %param.44) | copy-start | bytes 8650756
  6.5 8.1 %copy-start.1 = (bf16[128,512]{1,0:T(8,128)(2,1)S(1)}, bf16[128,512]{1,0:T(8,128)(2,1)}, u32[]{:S(2)}) copy-start(bf16[128,512]{1,0:T(8,128)(2,1)} %param.23) | copy-start | bytes 393220
  6.5 8.1 %copy-start.10 = (f32[512]{0:T(512)S(1)}, f32[512]{0:T(512)}, u32[]{:S(2)}) copy-start(f32[512]{0:T(512)} %param.24) | copy-start | bytes 6148
  6.5 8.1 %copy-start.5 = (bf16[512,512]{1,0:T(8,128)(2,1)S(1)}, bf16[512,512]{1,0:T(8,128)(2,1)}, u32[]{:S(2)}) copy-start(bf16[512,512]{1,0:T(8,128)(2,1)} %param.27) | copy-start | bytes 1572868
  6.5 36.4 %reduce-scatter.16.cloned.1.call-start = ((), (), s32[]{:S(2)}) async-start(), calls=%async_computation.10 | async-start | bytes 73728
  8.5 28.2 %copy-start.22 = (f32[4]{0:T(128)S(1)}, f32[4]{0:T(128)}, u32[]{:S(2)}) copy-start(f32[4]{0:T(128)} %param.31) | copy-start | bytes 52
  8.5 66.2 %copy-start.31 = (f32[4]{0:T(128)S(1)}, f32[4]{0:T(128)}, u32[]{:S(2)}) copy-start(f32[4]{0:T(128)} %param.30) | copy-start | bytes 52
  8.5 65.3 %reduce-scatter.18.cloned.1.call-start = ((), (), s32[]{:S(2)}) async-start(), calls=%async_computation.11 | async-start | bytes 73728
  10.2 66.0 %copy-start.26 = (f32[16,4]{0,1:T(4,128)S(1)}, f32[16,4]{0,1:T(4,128)}, u32[]{:S(2)}) copy-start(f32[16,4]{0,1:T(4,128)} %param.34) | copy-start | bytes 772
  10.3 94.6 %reduce-scatter.10.cloned.1.call-start = ((), (), s32[]{:S(2)}) async-start(), calls=%async_computation.5 | async-start | bytes 294912 | tf_op jit(solution)/shard_map/reduce_scatter | solution.py:109
  12.4 123.5 %reduce-scatter.12.cloned.1.call-start = ((), (), s32[]{:S(2)}) async-start(), calls=%async_computation.6 | async-start | bytes 294912 | tf_op jit(solution)/shard_map/reduce_scatter | solution.py:110
  14.6 152.5 %reduce-scatter.14.cloned.1.call-start = ((), (), s32[]{:S(2)}) async-start(), calls=%async_computation.7 | async-start | bytes 294912 | tf_op jit(solution)/shard_map/reduce_scatter | solution.py:111
  15.6 227.4 %all-reduce.6.cloned.1.call-start = ((), (), s32[]{:S(2)}) async-start(), calls=%async_computation.8 | async-start | bytes 524288 | tf_op jit(solution)/shard_map/psum | solution.py:158
  36.7 131.8 %copy-start.24 = (f32[16]{0:T(128)}, f32[16]{0:T(128)S(1)}, u32[]{:S(2)}) copy-start(f32[16]{0:T(128)S(1)} %fusion.30) | copy-start | bytes 196
  37.6 130.9 %copy-start.17 = (f32[16,4]{0,1:T(4,128)}, f32[16,4]{0,1:T(4,128)S(1)}, u32[]{:S(2)}) copy-start(f32[16,4]{0,1:T(4,128)S(1)} %fusion.32) | copy-start | bytes 772
  43.8 124.7 %copy-start.14 = (f32[16,4]{0,1:T(4,128)}, f32[16,4]{0,1:T(4,128)S(1)}, u32[]{:S(2)}) copy-start(f32[16,4]{0,1:T(4,128)S(1)} %copy.64) | copy-start | bytes 772
  74.6 93.9 %copy-start.19 = (f32[16,4]{0,1:T(4,128)}, f32[16,4]{0,1:T(4,128)S(1)}, u32[]{:S(2)}) copy-start(f32[16,4]{0,1:T(4,128)S(1)} %copy.65) | copy-start | bytes 772
  170.8 4.9 %copy-start.3 = (bf16[16,4,128,128]{3,2,1,0:T(8,128)(2,1)S(1)}, bf16[16,4,128,128]{3,2,1,0:T(8,128)(2,1)}, u32[]{:S(2)}) copy-start(bf16[16,4,128,128]{3,2,1,0:T(8,128)(2,1)} %param.35) | copy-start | bytes 6291460
  175.8 24.9 %copy-start.6 = (bf16[512,512]{1,0:T(8,128)(2,1)S(1)}, bf16[512,512]{1,0:T(8,128)(2,1)}, u32[]{:S(2)}) copy-start(bf16[512,512]{1,0:T(8,128)(2,1)} %param.41) | copy-start | bytes 1572868
  184.2 2.3 copy-start.13
  184.2 2.3 copy-start.30
  201.6 119.3 %all-reduce.10.cloned.1.call-start = ((), (), s32[]{:S(2)}) async-start(), calls=%async_computation.12 | async-start | bytes 5767168 | tf_op jit(solution)/shard_map/psum | solution.py:164
  248.1 119.7 %all-reduce.8.cloned.1.call-start = ((), (), s32[]{:S(2)}) async-start(), calls=%async_computation.9 | async-start | bytes 524288 | tf_op jit(solution)/shard_map/psum | solution.py:167
  320.9 46.9 %copy-start.4 = (f32[128,512]{1,0:T(8,128)S(1)}, f32[128,512]{1,0:T(8,128)}, u32[]{:S(2)}) copy-start(f32[128,512]{1,0:T(8,128)} %all-reduce.6.cloned.1.call-done) | copy-start | bytes 786436
  (17 other events, 38.6 us)
Sparse Core Ops, SparseCore 0:
  9.6 33.3 reduce-scatter.15
  45.2 28.5 reduce-scatter.17
  76.0 28.8 reduce-scatter.9
  107.0 28.9 reduce-scatter.11
  138.0 28.9 reduce-scatter.13
  201.8 41.1 all-reduce.5
  248.2 72.6 all-reduce.9
  325.2 42.5 all-reduce.7
where the time goes:
time: 377 us; the launch traced here: 376 us
  waiting for transfers between devices  266 us (71%)
  blocking collectives  48.3 us (13%)
  matrix products  28 us (7%)
  between operations  14.5 us (4%)
  local copies, waits for them, and re-layouts  10.6 us (3%)
  other arithmetic  8.77 us (2%)
    psum x1, waiting for transfers between devices, body(): gate_sum, up_sum, mid_sum = lax.psum((gate_part, up_part, mid_square), 'tp')  56.5 us
    psum x1, waiting for transfers between devices, body(): mixed = lax.psum(down_part, 'kv')  42.7 us
    psum x1, waiting for transfers between devices, body(): attended = lax.psum(attended_part, 'kv')  41.3 us
    unnamed x10, waiting for transfers between devices  35.3 us
    reduce_scatter x1, waiting for transfers between devices, body(): lax.psum_scatter(partial_of(key_weight), 'tp', scatter_dimension=0, tiled...  31.1 us
    reduce_scatter x1, waiting for transfers between devices, body(): lax.psum_scatter(partial_of(value_weight), 'tp', scatter_dimension=0, til...  31.1 us
    reduce_scatter x1, waiting for transfers between devices, body(): lax.psum_scatter(partial_of(query_weight), 'tp', scatter_dimension=0, til...  27.9 us
    unnamed x1, blocking collectives  18.1 us
  transfers between devices with their start and end apart: 8, of which 8 were waited for; matrix products, arithmetic and copies ran while one was open for 4% of the time, Pallas kernels for 0%

commit v1 on v0

--- a/solution.py
+++ b/solution.py
@@ -5,6 +5,7 @@
 
 D = 4096
 epsilon = 1e-06
+recover_the_sections = lambda xin: jnp.sum(lax.all_gather(xin, "kv"), axis=0)
 
 
 def memory_cell(
@@ -155,7 +156,7 @@
         output_weight,
         preferred_element_type=jnp.float32,
     )
-    attended = lax.psum(attended_part, "kv")
+    attended = recover_the_sections(attended_part)
     res_wide = tok_wide + attended
     mid_square = jnp.sum(res_wide * res_wide, axis=1)
     mid_scaled = (res_wide * mixer_norm_gain).astype(jnp.bfloat16)

time: 377 us -> 361 us (0.958)
  waiting for transfers between devices: 266 us -> 249 us
    psum x1 -> x0, waiting for transfers between devices: 41.3 us -> none  [body(): attended = lax.psum(attended_part, 'kv')]
    all_gather x0 -> x1, waiting for transfers between devices: none -> 24.7 us  [lax.all_gather(xin, 'kv')]
where the time goes in v1:
time: 361 us; the launch traced here: 360 us
  waiting for transfers between devices  249 us (69%)
  blocking collectives  48.7 us (13%)
  matrix products  27.9 us (8%)
  between operations  14.6 us (4%)
  local copies, waits for them, and re-layouts  10.6 us (3%)
  other arithmetic  9.14 us (3%)
    psum x1, waiting for transfers between devices, body(): gate_sum, up_sum, mid_sum = lax.psum((gate_part, up_part, mid_square), 'tp')  56.1 us
    psum x1, waiting for transfers between devices, body(): mixed = lax.psum(down_part, 'kv')  42.7 us
    unnamed x10, waiting for transfers between devices  35.3 us
    reduce_scatter x1, waiting for transfers between devices, body(): lax.psum_scatter(partial_of(key_weight), 'tp', scatter_dimension=0, tiled...  31.1 us
    reduce_scatter x1, waiting for transfers between devices, body(): lax.psum_scatter(partial_of(value_weight), 'tp', scatter_dimension=0, til...  31.1 us
    reduce_scatter x1, waiting for transfers between devices, body(): lax.psum_scatter(partial_of(query_weight), 'tp', scatter_dimension=0, til...  27.9 us
    all_gather x1, waiting for transfers between devices, lax.all_gather(xin, 'kv')  24.7 us
    unnamed x1, blocking collectives  18.1 us
  transfers between devices with their start and end apart: 8, of which 8 were waited for; matrix products, arithmetic and copies ran while one was open for 4% of the time, Pallas kernels for 0%

profile of v1, /device:TPU:0, one launch (start us, length us, event | category | flops | bytes accessed | tf_op | source)
XLA Modules:
  0.0 360.2 jit_solution(15451674183434411174)
XLA Ops:
  6.6 1.9 fusion.16
  8.5 1.7 fusion.14
  10.3 2.1 fusion.12
  12.5 2.1 fusion.10
  15.8 18.1 %all-reduce = f32[128]{0:T(128)S(1)} all-reduce(f32[128]{0:T(128)S(1)} %fusion.4), channel_id=4, replica_groups=mesh['kv'=4,'tp'=8] {'tp'}, use_global_device_ids=true, to_apply=%region_2.0.clone | all-reduce | flops 128 | bytes 1024
  37.7 5.3 %reduce-scatter.16.cloned.1.call-done = f32[16,16]{1,0:T(8,128)} async-done(((f32[128,16]{1,0:T(8,128)}), f32[16,16]{1,0:T(8,128)}) %reduce-scatter.16.cloned.1.call-update) | async-done | bytes 1040
  43.9 29.9 %reduce-scatter.18.cloned.1.call-done = f32[16,16]{1,0:T(8,128)} async-done(((f32[128,16]{1,0:T(8,128)}), f32[16,16]{1,0:T(8,128)}) %reduce-scatter.18.cloned.1.call-update) | async-done | bytes 1040
  74.6 1.6 fusion.34
  76.9 27.9 %reduce-scatter.10.cloned.1.call-done = f32[16,512]{1,0:T(8,128)} async-done(((f32[128,512]{1,0:T(8,128)}), f32[16,512]{1,0:T(8,128)}) %reduce-scatter.10.cloned.1.call-update) | async-done | bytes 32784 | tf_op jit(solution)/shard_map/reduce_scatter | solution.py:110
  104.9 31.1 %reduce-scatter.12.cloned.1.call-done = f32[16,512]{1,0:T(8,128)} async-done(((f32[128,512]{1,0:T(8,128)}), f32[16,512]{1,0:T(8,128)}) %reduce-scatter.12.cloned.1.call-update) | async-done | bytes 32784 | tf_op jit(solution)/shard_map/reduce_scatter | solution.py:111
  136.0 31.1 %reduce-scatter.14.cloned.1.call-done = f32[16,512]{1,0:T(8,128)} async-done(((f32[128,512]{1,0:T(8,128)}), f32[16,512]{1,0:T(8,128)}) %reduce-scatter.14.cloned.1.call-update) | async-done | bytes 32784 | tf_op jit(solution)/shard_map/reduce_scatter | solution.py:112
  167.0 1.5 fusion.25
  170.8 4.9 %fusion.36 = f32[16,4,1,128]{3,2,1,0:T(1,128)} fusion(bf16[16,4,128,1]{2,3,1,0:T(2,128)(2,1)S(1)} %reshape.55, f32[16,4,128,128]{3,2,1,0:T(8,128)} %param.32), kind=kOutput, calls=%fused_computation.61 | convolution fusion | flops 12582912 | bytes 4243456 | tf_op jit(solution)/shard_map/bhkv,bhk->bhv/dot_general | solution.py:54
  175.8 2.0 fusion.35
  184.2 2.3 fusion.22
  186.7 14.0 %all_gather.9 = bf16[128,512]{1,0:T(8,128)(2,1)S(1)} all-gather(bf16[16,512]{1,0:T(8,128)(2,1)S(1)} %bitcast.47), channel_id=1, replica_groups=mesh['kv'=4,'tp'=8] {'tp'}, dimensions={0}, use_global_device_ids=true | all-gather | bytes 147456 | tf_op jit(solution)/shard_map/all_gather | solution.py:155
  201.7 24.7 %all-gather.3.cloned.1.call-done = f32[512,512]{1,0:T(8,128)} async-done(((f32[128,512]{1,0:T(8,128)}), f32[512,512]{1,0:T(8,128)}) %all-gather.3.cloned.1.call-update) | async-done | bytes 1048592 | tf_op jit(solution)/shard_map/all_gather | solution.py:8
  227.9 1.7 fusion.39
  230.2 1.7 fusion.38
  232.0 16.6 %psum.29 = f32[128]{0:T(128)S(1)} all-reduce(f32[128]{0:T(128)S(1)} %get-tuple-element.12), channel_id=1, replica_groups=mesh['kv'=4,'tp'=8] {'tp'}, use_global_device_ids=true, to_apply=%region_15.16 | all-reduce | flops 128 | bytes 1024 | tf_op jit(solution)/shard_map/psum | solution.py:165
  248.7 56.1 %all-reduce.7.cloned.1.call-done = (f32[128,2816]{1,0:T(8,128)}, f32[128,2816]{1,0:T(8,128)}) async-done(((f32[128,2816]{1,0:T(8,128)}, f32[128,2816]{1,0:T(8,128)}), (f32[128,2816]{1,0:T(8,128)}, f32[128,2816]{1,0:T(8,128)})) %all-reduce.7.cloned.1.call-update) | async-done | bytes 2883600 | tf_op jit(solution)/shard_map/psum | solution.py:165
  304.8 4.1 %fusion.2 = f32[128,512]{1,0:T(8,128)} fusion(bf16[2816,512]{1,0:T(8,128)(2,1)} %param.45, f32[128,2816]{1,0:T(8,128)} %get-tuple-element.7, f32[128,2816]{1,0:T(8,128)} %get-tuple-element.8, f32[128]{0:T(128)S(1)} %add_rsqrt_fusion), kind=kOutput, calls=%fused_computation.4 | convolution fusion | flops 371982336 | bytes 6029824 | tf_op jit(solution)/shard_map/dot_general | solution.py:167
  308.9 42.7 %all-reduce.5.cloned.1.call-done = f32[128,512]{1,0:T(8,128)} async-done(((f32[128,512]{1,0:T(8,128)}), f32[128,512]{1,0:T(8,128)}) %all-reduce.5.cloned.1.call-update) | async-done | bytes 262160 | tf_op jit(solution)/shard_map/psum | solution.py:168
  351.6 1.7 fusion.5
  (112 shorter events, 18.9 us)
Async XLA Ops:
  6.5 221.4 %copy-start = (bf16[512,2816]{1,0:T(8,128)(2,1)S(1)}, bf16[512,2816]{1,0:T(8,128)(2,1)}, u32[]{:S(2)}) copy-start(bf16[512,2816]{1,0:T(8,128)(2,1)} %param.44) | copy-start | bytes 8650756
  6.5 8.1 %copy-start.1 = (bf16[128,512]{1,0:T(8,128)(2,1)S(1)}, bf16[128,512]{1,0:T(8,128)(2,1)}, u32[]{:S(2)}) copy-start(bf16[128,512]{1,0:T(8,128)(2,1)} %param.23) | copy-start | bytes 393220
  6.5 8.1 %copy-start.9 = (f32[512]{0:T(512)S(1)}, f32[512]{0:T(512)}, u32[]{:S(2)}) copy-start(f32[512]{0:T(512)} %param.24) | copy-start | bytes 6148
  6.5 8.1 %copy-start.4 = (bf16[512,512]{1,0:T(8,128)(2,1)S(1)}, bf16[512,512]{1,0:T(8,128)(2,1)}, u32[]{:S(2)}) copy-start(bf16[512,512]{1,0:T(8,128)(2,1)} %param.27) | copy-start | bytes 1572868
  6.5 36.4 %reduce-scatter.16.cloned.1.call-start = ((), (), s32[]{:S(2)}) async-start(), calls=%async_computation.10 | async-start | bytes 73728
  8.5 28.2 %copy-start.21 = (f32[4]{0:T(128)S(1)}, f32[4]{0:T(128)}, u32[]{:S(2)}) copy-start(f32[4]{0:T(128)} %param.31) | copy-start | bytes 52
  8.5 66.2 %copy-start.31 = (f32[4]{0:T(128)S(1)}, f32[4]{0:T(128)}, u32[]{:S(2)}) copy-start(f32[4]{0:T(128)} %param.30) | copy-start | bytes 52
  8.5 65.3 %reduce-scatter.18.cloned.1.call-start = ((), (), s32[]{:S(2)}) async-start(), calls=%async_computation.11 | async-start | bytes 73728
  10.2 66.0 %copy-start.25 = (f32[16,4]{0,1:T(4,128)S(1)}, f32[16,4]{0,1:T(4,128)}, u32[]{:S(2)}) copy-start(f32[16,4]{0,1:T(4,128)} %param.34) | copy-start | bytes 772
  10.3 94.6 %reduce-scatter.10.cloned.1.call-start = ((), (), s32[]{:S(2)}) async-start(), calls=%async_computation.5 | async-start | bytes 294912 | tf_op jit(solution)/shard_map/reduce_scatter | solution.py:110
  12.4 123.5 %reduce-scatter.12.cloned.1.call-start = ((), (), s32[]{:S(2)}) async-start(), calls=%async_computation.6 | async-start | bytes 294912 | tf_op jit(solution)/shard_map/reduce_scatter | solution.py:111
  14.6 152.5 %reduce-scatter.14.cloned.1.call-start = ((), (), s32[]{:S(2)}) async-start(), calls=%async_computation.7 | async-start | bytes 294912 | tf_op jit(solution)/shard_map/reduce_scatter | solution.py:112
  15.6 210.8 %all-gather.3.cloned.1.call-start = ((), (), s32[]{:S(2)}) async-start(), calls=%async_computation.9 | async-start | bytes 1310720 | tf_op jit(solution)/shard_map/all_gather | solution.py:8
  36.7 131.8 %copy-start.23 = (f32[16]{0:T(128)}, f32[16]{0:T(128)S(1)}, u32[]{:S(2)}) copy-start(f32[16]{0:T(128)S(1)} %fusion.30) | copy-start | bytes 196
  37.6 130.9 %copy-start.16 = (f32[16,4]{0,1:T(4,128)}, f32[16,4]{0,1:T(4,128)S(1)}, u32[]{:S(2)}) copy-start(f32[16,4]{0,1:T(4,128)S(1)} %fusion.32) | copy-start | bytes 772
  43.8 124.7 %copy-start.13 = (f32[16,4]{0,1:T(4,128)}, f32[16,4]{0,1:T(4,128)S(1)}, u32[]{:S(2)}) copy-start(f32[16,4]{0,1:T(4,128)S(1)} %copy.64) | copy-start | bytes 772
  74.6 93.9 %copy-start.18 = (f32[16,4]{0,1:T(4,128)}, f32[16,4]{0,1:T(4,128)S(1)}, u32[]{:S(2)}) copy-start(f32[16,4]{0,1:T(4,128)S(1)} %copy.65) | copy-start | bytes 772
  170.8 4.9 %copy-start.3 = (bf16[16,4,128,128]{3,2,1,0:T(8,128)(2,1)S(1)}, bf16[16,4,128,128]{3,2,1,0:T(8,128)(2,1)}, u32[]{:S(2)}) copy-start(bf16[16,4,128,128]{3,2,1,0:T(8,128)(2,1)} %param.35) | copy-start | bytes 6291460
  175.8 24.9 %copy-start.5 = (bf16[512,512]{1,0:T(8,128)(2,1)S(1)}, bf16[512,512]{1,0:T(8,128)(2,1)}, u32[]{:S(2)}) copy-start(bf16[512,512]{1,0:T(8,128)(2,1)} %param.41) | copy-start | bytes 1572868
  184.2 2.4 copy-start.12
  184.2 2.4 copy-start.29
  186.5 41.3 %copy-start.30 = (f32[512]{0:T(512)S(1)}, f32[512]{0:T(512)}, u32[]{:S(2)}) copy-start(f32[512]{0:T(512)} %param.42) | copy-start | bytes 6148
  201.6 103.1 %all-reduce.7.cloned.1.call-start = ((), (), s32[]{:S(2)}) async-start(), calls=%async_computation.12 | async-start | bytes 5767168 | tf_op jit(solution)/shard_map/psum | solution.py:165
  232.0 119.7 %all-reduce.5.cloned.1.call-start = ((), (), s32[]{:S(2)}) async-start(), calls=%async_computation.8 | async-start | bytes 524288 | tf_op jit(solution)/shard_map/psum | solution.py:168
  (17 other events, 38.6 us)
Sparse Core Ops, SparseCore 0:
  9.6 33.3 reduce-scatter.15
  45.2 28.5 reduce-scatter.17
  76.0 28.8 reduce-scatter.9
  107.0 28.9 reduce-scatter.11
  138.0 28.9 reduce-scatter.13
  201.8 24.6 all-gather.2
  232.1 72.6 all-reduce.6
  309.0 42.5 all-reduce.4
